TPU v7x, 32 devices: a whole 2x2x4 slice. The times are simulated.
32 devices in a mesh: kv: 8 (over z, y), tp: 4 (over x, core).
Axes of the slice: x: 2, y: 2, z: 4, core: 2. Of those that a mesh axis runs over, the one named last changes fastest.
Arguments:
- tokens: bfloat16 [16, 16, 4096], replicated, may hold values from -6 to 6
- gain_pre: float32 [4096], replicated, may hold values from 0.1 to 1.9
- w_query: bfloat16 [4096, 2048], P('kv', 'tp'), may hold values from -0.09375 to 0.09375
- w_key: bfloat16 [4096, 2048], P('kv', 'tp'), may hold values from -0.09375 to 0.09375
- w_value: bfloat16 [4096, 2048], P('kv', 'tp'), may hold values from -0.09375 to 0.09375
- w_forget: bfloat16 [4096, 16], replicated, may hold values from -0.09375 to 0.09375
- b_forget: float32 [16], replicated
- w_out: bfloat16 [2048, 4096], P('tp', 'kv'), may hold values from -0.125 to 0.125
- gain_post: float32 [4096], P(('kv', 'tp')), may hold values from 0.1 to 1.9
- key_cache: bfloat16 [16, 1024, 16, 128], P(None, 'kv', 'tp'), may hold values from -6 to 6
- value_cache: bfloat16 [16, 1024, 16, 128], P(None, 'kv', 'tp'), may hold values from -6 to 6
- cum_cache: float32 [16, 1024, 16], P(None, 'kv', 'tp'), may hold values from -402 to 0, as said below
- lengths: int32 [16], replicated, may hold values from 512 to 992
- accepted: int32 [16], replicated, may hold values from 0 to 16
- parent: int32 [16, 16], replicated, may hold values from -1 to 14, as said below
Outputs:
- mixed: bfloat16 [16, 16, 4096], P(None, None, ('kv', 'tp'))
- key_out: bfloat16 [16, 1024, 16, 128], P(None, 'kv', 'tp')
- value_out: bfloat16 [16, 1024, 16, 128], P(None, 'kv', 'tp')
- cum_out: float32 [16, 1024, 16], P(None, 'kv', 'tp')
Inputs may be any that keep to these rules, and one draw needn't show every extreme that they name: parent[s, 0] is -1 and parent[s, i] lies between -1 and i - 1. `cum_cache`: along the positions of each sequence and head the values never rise. lengths + accepted + 16 never exceeds 1024.
All inputs are finite; a program needn't handle non-finite values.
Results may differ from a plain program's by a relative error of at most 0.03.
Values may be sent and summed in bfloat16 or wider, within the bound.
No kernel may reach another device: no remote copies, remote signals or barrier semaphores. Data moves between devices by JAX's collectives and lax.ppermute only.
A program may use at most 64 MiB of HBM per device.

v0:
```python
import jax
import jax.numpy as jnp
from jax import lax
from jax.sharding import PartitionSpec as P

epsilon = 1e-06
floor_value = -1e30


def merged(part, axis, combine):
    gathered = jax.tree.map(lambda a: lax.all_gather(a, axis), part)

    def take(source):
        return jax.tree.map(lambda a: lax.dynamic_index_in_dim(a, source, 0, False), gathered)

    return lax.fori_loop(
        1, lax.axis_size(axis), lambda source, state: combine(state, take(source)), take(0)
    )


def ancestry(parent_ids, members):
    identity = jnp.eye(members, dtype=jnp.float32)
    parent_hot = (
        parent_ids[:, :, None] == jnp.arange(members, dtype=jnp.int32)[None, None, :]
    ).astype(jnp.float32)
    ancestors = jnp.minimum(identity[None] + parent_hot, 1.0)
    for sweep in range(max(1, (members - 1).bit_length())):
        ancestors = jnp.minimum(
            jnp.einsum("bij,bjk->bik", ancestors, ancestors, precision=lax.Precision.HIGHEST), 1.0
        )
    return ancestors


def combine_parts(first, second):
    new_max = jnp.maximum(first[0], second[0])
    first_scale = jnp.exp(first[0] - new_max)
    second_scale = jnp.exp(second[0] - new_max)
    return (
        new_max,
        first[1] * first_scale + second[1] * second_scale,
        first[2] * first_scale[..., None] + second[2] * second_scale[..., None],
        jnp.maximum(first[3], second[3]),
    )


def finish_rows(cache_max, cache_total, cache_values, last_rows, tree_max, tree_total, tree_values):
    shifted = cache_max + last_rows
    top = jnp.maximum(shifted, tree_max)
    cache_scale = jnp.exp(shifted - top)
    tree_scale = jnp.exp(tree_max - top)
    attended = (
        (cache_values * cache_scale[..., None] + tree_values * tree_scale[..., None])
        / (cache_total * cache_scale + tree_total * tree_scale)[..., None]
    ).astype(jnp.bfloat16)
    return attended.reshape(attended.shape[0], attended.shape[1] * attended.shape[2])


def per_device(
    tokens,
    gain_pre,
    w_query,
    w_key,
    w_value,
    w_forget,
    b_forget,
    w_out,
    gain_post,
    key_cache,
    value_cache,
    cum_cache,
    lengths,
    accepted,
    parent,
):
    num_seqs, proposals, model_width = tokens.shape
    kv_rank = lax.axis_index("kv")
    tp_rank = lax.axis_index("tp")
    span = key_cache.shape[1]
    heads_local = key_cache.shape[2]
    head_dim = key_cache.shape[3]
    scale = head_dim ** (-0.5)
    all_rows = num_seqs * proposals
    tok_float = tokens.astype(jnp.float32)
    normed = (
        tok_float
        * lax.rsqrt(jnp.mean(tok_float * tok_float, -1, keepdims=True) + epsilon)
        * gain_pre
    ).astype(jnp.bfloat16)
    flat = normed.reshape(all_rows, model_width)
    weight_rows = w_query.shape[0]
    local_rows = lax.dynamic_slice_in_dim(flat, kv_rank * weight_rows, weight_rows, 1)
    query_part = jnp.dot(local_rows, w_query, preferred_element_type=jnp.float32)
    key_part = jnp.dot(local_rows, w_key, preferred_element_type=jnp.float32)
    value_part = jnp.dot(local_rows, w_value, preferred_element_type=jnp.float32)
    summed = (
        lax.psum(query_part.astype(jnp.bfloat16), "kv").astype(jnp.float32),
        lax.psum(key_part.astype(jnp.bfloat16), "kv").astype(jnp.float32),
        lax.psum(value_part.astype(jnp.bfloat16), "kv").astype(jnp.float32),
    )
    query_flat = summed[0].astype(jnp.bfloat16)
    key_flat = summed[1].astype(jnp.bfloat16)
    value_flat = summed[2].astype(jnp.bfloat16)
    query = query_flat.reshape(num_seqs, proposals, heads_local, head_dim)
    key_new = key_flat.reshape(num_seqs, proposals, heads_local, head_dim)
    value_new = value_flat.reshape(num_seqs, proposals, heads_local, head_dim)
    forget_cols = lax.dynamic_slice_in_dim(w_forget, tp_rank * heads_local, heads_local, 1)
    forget_bias = lax.dynamic_slice_in_dim(b_forget, tp_rank * heads_local, heads_local, 0)
    log_forget = jax.nn.log_sigmoid(
        jnp.dot(flat, forget_cols, preferred_element_type=jnp.float32) + forget_bias
    ).reshape(num_seqs, proposals, heads_local)
    ancestors = ancestry(parent, proposals)
    path = jnp.einsum("bij,bjh->bih", ancestors, log_forget, precision=lax.Precision.HIGHEST)
    valid = lengths + accepted
    positions = kv_rank * span + jnp.arange(span, dtype=jnp.int32)
    live = (positions[None, :] < valid[:, None])[:, None, None, :]
    score = (
        jnp.einsum("bihd,bkhd->bihk", query, key_cache, preferred_element_type=jnp.float32) * scale
        + path[..., None]
        - jnp.swapaxes(cum_cache, 1, 2)[:, None]
    )
    block_max = jnp.max(jnp.where(live, score, floor_value), axis=-1)
    weight = jnp.exp(jnp.where(live, score - block_max[..., None], floor_value))
    block_total = jnp.sum(weight, axis=-1)
    block_values = jnp.einsum(
        "bihk,bkhd->bihd",
        weight.astype(jnp.bfloat16),
        value_cache,
        preferred_element_type=jnp.float32,
    )
    owner = positions[None, :] == (valid - 1)[:, None]
    candidate = jnp.max(jnp.where(owner[:, :, None], cum_cache, floor_value), axis=1)
    tree_mask = (ancestors > 0.5)[:, :, None, :]
    tree_score = (
        jnp.einsum("bihd,bjhd->bihj", query, key_new, preferred_element_type=jnp.float32) * scale
        + path[..., None]
        - jnp.swapaxes(path, 1, 2)[:, None]
    )
    tree_max = jnp.max(jnp.where(tree_mask, tree_score, floor_value), axis=-1)
    tree_weight = jnp.exp(jnp.where(tree_mask, tree_score - tree_max[..., None], floor_value))
    tree_total = jnp.sum(tree_weight, axis=-1)
    tree_values = jnp.einsum(
        "bihj,bjhd->bihd",
        tree_weight.astype(jnp.bfloat16),
        value_new,
        preferred_element_type=jnp.float32,
    )
    tree_max_rows = tree_max.reshape(all_rows, heads_local)
    tree_total_rows = tree_total.reshape(all_rows, heads_local)
    tree_values_rows = tree_values.reshape(all_rows, heads_local, head_dim)
    cache_max, cache_total, cache_values, last_cum = merged(
        (block_max, block_total, block_values, candidate), "kv", combine_parts
    )
    last_rows = jnp.broadcast_to(last_cum[:, None, :], (num_seqs, proposals, heads_local)).reshape(
        all_rows, heads_local
    )
    attended = finish_rows(
        cache_max.reshape(all_rows, heads_local),
        cache_total.reshape(all_rows, heads_local),
        cache_values.reshape(all_rows, heads_local, head_dim),
        last_rows,
        tree_max_rows,
        tree_total_rows,
        tree_values_rows,
    )
    mixed_part = jnp.dot(attended, w_out, preferred_element_type=jnp.float32)
    mixed_sum = lax.psum_scatter(
        mixed_part.astype(jnp.bfloat16), "tp", scatter_dimension=1, tiled=True
    ).astype(jnp.float32)
    squares = lax.psum(jnp.sum(mixed_sum * mixed_sum, axis=1), ("kv", "tp"))
    mixed = (mixed_sum * lax.rsqrt(squares / model_width + epsilon)[:, None] * gain_post).astype(
        jnp.bfloat16
    )
    mixed = mixed.reshape(num_seqs, proposals, mixed_sum.shape[1])
    relative = positions[None, :] - valid[:, None]
    select = relative[:, :, None] == jnp.arange(proposals, dtype=jnp.int32)[None, None, :]
    written = (relative >= 0) & (relative < proposals)
    placed_keys = jnp.einsum(
        "bkj,bjhd->bkhd", select.astype(jnp.bfloat16), key_new, preferred_element_type=jnp.float32
    ).astype(jnp.bfloat16)
    placed_values = jnp.einsum(
        "bkj,bjhd->bkhd", select.astype(jnp.bfloat16), value_new, preferred_element_type=jnp.float32
    ).astype(jnp.bfloat16)
    key_out = jnp.where(written[:, :, None, None], placed_keys, key_cache)
    value_out = jnp.where(written[:, :, None, None], placed_values, value_cache)
    cum_new = last_cum[:, None, :] + path
    placed_cum = jnp.einsum(
        "bkj,bjh->bkh", select.astype(jnp.float32), cum_new, precision=lax.Precision.HIGHEST
    )
    cum_out = jnp.where(written[:, :, None], placed_cum, cum_cache)
    return (mixed, key_out, value_out, cum_out)


def solution(mesh):
    return jax.shard_map(
        per_device,
        mesh=mesh,
        in_specs=(
            P(),
            P(),
            P("kv", "tp"),
            P("kv", "tp"),
            P("kv", "tp"),
            P(),
            P(),
            P("tp", "kv"),
            P(("kv", "tp")),
            P(None, "kv", "tp", None),
            P(None, "kv", "tp", None),
            P(None, "kv", "tp"),
            P(),
            P(),
            P(),
        ),
        out_specs=(
            P(None, None, ("kv", "tp")),
            P(None, "kv", "tp", None),
            P(None, "kv", "tp", None),
            P(None, "kv", "tp"),
        ),
        check_vma=False,
    )
```

profile of v0, /device:TPU:0, one launch (start us, length us, event | category | flops | bytes accessed | tf_op | source)
XLA Modules:
  0.0 293.7 jit_solution(18166977951993972896)
XLA Ops:
  7.2 2.1 fusion.4
  9.4 2.2 fusion.6
  12.8 1.3 convolution_convert_fusion.1
  14.2 1.4 convolution_convert_fusion.3
  18.0 1.5 fusion.71
  20.6 75.1 %all-reduce.3.cloned.1.call-done = (bf16[16,16,4,128]{3,1,2,0:T(8,128)(2,1)}, bf16[16,16,4,128]{3,1,2,0:T(8,128)(2,1)}, bf16[16,16,4,128]{3,1,2,0:T(8,128)(2,1)}) async-done(((bf16[16,16,4,128]{3,1,2,0:T(8,128)(2,1)}, bf16[16,16,4,128]{3,1,2,0:T(8,128)(2,1)}, bf16[16,16,4,128]{3,1,2,0:T(8,128)(2,1)}), (bf16[16,16,4,128]{3,1,2,0:T(8,128)(2,1)}, bf16[16,16,4,128]{3,1,2,0:T(8,128)(2,1)}, ...) | async-done | bytes 786448 | tf_op jit(solution)/shard_map/psum | solution.py:97
  95.7 3.0 %select_reduce_fusion.1 = (f32[16,16,4]{1,2,0:T(4,128)S(1)}, f32[16,16,4,128]{3,1,2,0:T(8,128)S(1)}) fusion(pred[16,128]{1,0:T(8,128)(4,1)S(1)} %get-tuple-element.314, f32[16,4,128]{2,1,0:T(4,128)S(1)} %bitcast.132, f32[16,16,4]{1,2,0:T(4,128)S(1)} %fusion.63, bf16[16,16,4,128]{3,1,2,0:T(8,128)(2,1)} %get-tuple-element.302, ...), kind=kOutput, calls=%fused_computation.51 | convolution fusion | flops 34208768 | bytes 2926592 | tf_op jit(solution)/shard_map/bihd,bkhd->bihk/dot_general | solution.py:117
  99.5 1.5 fusion.11
  101.4 26.7 %all-gather.4 = f32[8,16,4]{1,2,0:T(4,128)S(1)} all-gather(f32[1,16,4]{1,2,0:T(4,128)S(1)} %bitcast.134), channel_id=5, replica_groups=mesh['kv'=8,'tp'=4] {'kv'}, dimensions={0}, use_global_device_ids=true | all-gather | bytes 2304 | tf_op jit(solution)/shard_map/all_gather | solution.py:11
  128.8 1.4 select_reduce_fusion
  131.9 32.2 %all-gather = f32[128,16,4]{1,2,0:T(4,128)S(1)} all-gather(f32[16,16,4]{1,2,0:T(4,128)S(1)} %get-tuple-element.320), channel_id=2, replica_groups=mesh['kv'=8,'tp'=4] {'kv'}, dimensions={0}, use_global_device_ids=true | all-gather | bytes 36864 | tf_op jit(solution)/shard_map/all_gather | solution.py:11
  164.1 1.5 fusion.33
  165.6 31.7 %all-gather.1 = f32[128,16,4]{1,2,0:T(4,128)S(1)} all-gather(f32[16,16,4]{1,2,0:T(4,128)S(1)} %fusion.33), channel_id=3, replica_groups=mesh['kv'=8,'tp'=4] {'kv'}, dimensions={0}, use_global_device_ids=true | all-gather | bytes 36864 | tf_op jit(solution)/shard_map/all_gather | solution.py:11
  198.3 3.1 %copy.110 = bf16[16,128,4,128]{3,2,1,0:T(4,128)(2,1)} copy(bf16[16,128,4,128]{3,1,2,0:T(8,128)(2,1)S(1)} %convert_select_fusion) | data formatting | bytes 4194304
  202.6 22.1 %while.21 = (s32[]{:T(128)}, f32[16,16,4]{1,2,0:T(4,128)S(1)}, f32[16,16,4]{1,2,0:T(4,128)S(1)}, f32[16,16,4,128]{3,2,1,0:T(4,128)S(1)}, f32[16,4]{0,1:T(4,128)S...) while((s32[]{:T(128)}, f32[16,16,4]{1,2,0:T(4,128)S(1)}, ...), condition=%wide.region_6.7_spmd, body=%wide.region_5.6_spmd.sunk | while | flops 399429 | bytes 2679715 | solution.py:16
  203.8 1.1 constant_dynamic-slice_fusion.2
  206.9 1.1 constant_dynamic-slice_fusion.2
  210.1 1.1 constant_dynamic-slice_fusion.2
  213.2 1.1 constant_dynamic-slice_fusion.2
  216.4 1.1 constant_dynamic-slice_fusion.2
  227.8 2.4 convert_select_fusion.1
  230.2 3.1 %copy.109 = bf16[16,128,4,128]{3,2,1,0:T(4,128)(2,1)} copy(bf16[16,128,4,128]{3,1,2,0:T(8,128)(2,1)S(1)} %convert_select_fusion.1) | data formatting | bytes 4194304
  234.2 11.8 %reduce-scatter.4.cloned.1.call-done = bf16[128,256]{1,0:T(8,128)(2,1)} async-done(((bf16[512,256]{1,0:T(8,128)(2,1)}), bf16[128,256]{1,0:T(8,128)(2,1)}) %reduce-scatter.4.cloned.1.call-update) | async-done | bytes 65552
  247.1 39.3 %psum.31 = f32[256]{0:T(256)S(1)} all-reduce(f32[256]{0:T(256)S(1)} %fusion.48), channel_id=1, replica_groups=mesh['kv'=8,'tp'=4] {'kv','tp'}, use_global_device_ids=true, to_apply=%region_13.14 | all-reduce | flops 256 | bytes 2048 | tf_op jit(solution)/shard_map/psum | solution.py:169
  (138 shorter events, 32.6 us)
Async XLA Ops:
  7.2 4.5 %copy-start = (bf16[512,512]{1,0:T(8,128)(2,1)S(1)}, bf16[512,512]{1,0:T(8,128)(2,1)}, u32[]{:S(2)}) copy-start(bf16[512,512]{1,0:T(8,128)(2,1)} %param.20) | copy-start | bytes 1572868
  7.2 2.2 copy-start.10
  7.2 88.5 %all-reduce.3.cloned.1.call-start = ((), (), s32[]{:S(2)}) async-start(), calls=%async_computation.3 | async-start | bytes 1572864 | tf_op jit(solution)/shard_map/psum | solution.py:97
  14.1 3.2 %copy-start.17 = (s32[16,16]{1,0:T(8,128)S(1)}, s32[16,16]{1,0:T(8,128)}, u32[]{:S(2)}) copy-start(s32[16,16]{1,0:T(8,128)} %param.31) | copy-start | bytes 3076
  14.1 3.8 %copy-start.18 = (f32[16]{0:T(128)S(1)}, f32[16]{0:T(128)}, u32[]{:S(2)}) copy-start(f32[16]{0:T(128)} %param.23) | copy-start | bytes 196
  14.1 3.9 %copy-start.13 = (s32[16]{0:T(128)S(1)}, s32[16]{0:T(128)}, u32[]{:S(2)}) copy-start(s32[16]{0:T(128)} %param.29) | copy-start | bytes 196
  14.1 3.9 %copy-start.14 = (s32[16]{0:T(128)S(1)}, s32[16]{0:T(128)}, u32[]{:S(2)}) copy-start(s32[16]{0:T(128)} %param.30) | copy-start | bytes 196
  17.2 78.5 %copy-start.6 = (f32[16,128,4]{1,2,0:T(4,128)S(1)}, f32[16,128,4]{1,2,0:T(4,128)}, u32[]{:S(2)}) copy-start(f32[16,128,4]{1,2,0:T(4,128)} %param.28) | copy-start | bytes 98308
  17.2 184.2 %all-gather.7.cloned.1.call-start = ((), (), s32[]{:S(2)}) async-start(), calls=%async_computation.1 | async-start | bytes 4718592 | tf_op jit(solution)/shard_map/all_gather | solution.py:11
  19.7 79.8 %copy-start.1 = (bf16[16,128,4,128]{3,2,1,0:T(4,128)(2,1)S(1)}, bf16[16,128,4,128]{3,2,1,0:T(4,128)(2,1)}, u32[]{:S(2)}) copy-start(bf16[16,128,4,128]{3,2,1,0:T(4,128)(2,1)} %param.27) | copy-start | bytes 6291460
  20.5 108.2 %copy-start.8 = (f32[16,16,4]{1,2,0:T(4,128)}, f32[16,16,4]{1,2,0:T(4,128)S(1)}, u32[]{:S(2)}) copy-start(f32[16,16,4]{1,2,0:T(4,128)S(1)} %fusion.63) | copy-start | bytes 12292
  98.7 0.8 copy-start.2
  99.5 30.7 %copy-start.4 = (bf16[16,16,4,128]{3,1,2,0:T(8,128)(2,1)S(1)}, bf16[16,16,4,128]{3,1,2,0:T(8,128)(2,1)}, u32[]{:S(2)}) copy-start(bf16[16,16,4,128]{3,1,2,0:T(8,128)(2,1)} %get-tuple-element.303) | copy-start | bytes 786436
  101.0 144.9 %reduce-scatter.4.cloned.1.call-start = ((), (), s32[]{:S(2)}) async-start(), calls=%async_computation.2 | async-start | bytes 327680
  128.1 0.7 copy-start.5
  130.2 67.0 %copy-start.11 = (s32[16,128]{1,0:T(8,128)S(1)}, s32[16,128]{1,0:T(8,128)}, u32[]{:S(2)}) copy-start(s32[16,128]{1,0:T(8,128)} %broadcast_subtract_fusion) | copy-start | bytes 24580
  224.7 1.9 copy-start.3
  224.8 1.8 copy-start.15
  226.6 1.2 copy-start.16
  230.2 3.1 %copy-start.7 = (f32[16,128,4]{1,2,0:T(4,128)S(1)}, f32[16,128,4]{1,2,0:T(4,128)}, u32[]{:S(2)}) copy-start(f32[16,128,4]{1,2,0:T(4,128)} %param.28) | copy-start | bytes 98308
  230.2 3.1 %copy-start.9 = (f32[16,16,4]{1,2,0:T(4,128)S(1)}, f32[16,16,4]{1,2,0:T(4,128)}, u32[]{:S(2)}) copy-start(f32[16,16,4]{1,2,0:T(4,128)} %copy-done.8) | copy-start | bytes 12292
  230.2 56.1 %copy-start.12 = (f32[128]{0:T(128)S(1)}, f32[128]{0:T(128)}, u32[]{:S(2)}) copy-start(f32[128]{0:T(128)} %param.25) | copy-start | bytes 1540
Sparse Core Ops, SparseCore 0:
  17.3 78.3 all-reduce.2
  101.2 77.8 all-gather.6
  228.0 17.9 reduce-scatter.3
where the time goes:
time: 295 us; the launch traced here: 294 us
  blocking collectives  130 us (44%)
  waiting for transfers between devices  87 us (29%)
  local copies, waits for them, and re-layouts  25.7 us (9%)
  other arithmetic  19.7 us (7%)
  matrix products  16.7 us (6%)
  between operations  14.2 us (5%)
    all_gather x3, blocking collectives, merged(): gathered = jax.tree.map(lambda a: lax.all_gather(a, axis), part)  90.6 us
    psum x1, waiting for transfers between devices, per_device(): lax.psum(key_part.astype(jnp.bfloat16), 'kv').astype(jnp.float32)  75.1 us
    psum x1, blocking collectives, per_device(): squares = lax.psum(jnp.sum(mixed_sum * mixed_sum, axis=1), ('kv', 'tp'))  39.3 us
    unnamed x4, waiting for transfers between devices  11.8 us
    unnamed x42, local copies, waits for them, and re-layouts  8.8 us
    dynamic_slice x11, local copies, waits for them, and re-layouts, take(): lax.dynamic_index_in_dim(a, source, 0, False)  8.64 us
    add x7, other arithmetic, combine_parts(): first[2] * first_scale[..., None] + second[2] * second_scale[..., None]  6.66 us
  transfers between devices with their start and end apart: 3, of which 2 were waited for; matrix products, arithmetic and copies ran while one was open for 7% of the time, Pallas kernels for 0%

commit v1 on v0

--- a/solution.py
+++ b/solution.py
@@ -166,7 +166,7 @@
     mixed_sum = lax.psum_scatter(
         mixed_part.astype(jnp.bfloat16), "tp", scatter_dimension=1, tiled=True
     ).astype(jnp.float32)
-    squares = lax.psum(jnp.sum(mixed_sum * mixed_sum, axis=1), ("kv", "tp"))
+    squares = jnp.sum(lax.all_gather(jnp.sum(mixed_sum * mixed_sum, axis=1), ("kv", "tp")), axis=0)
     mixed = (mixed_sum * lax.rsqrt(squares / model_width + epsilon)[:, None] * gain_post).astype(
         jnp.bfloat16
     )

time: 295 us -> 296 us (level)
    all_gather x0 -> x1, blocking collectives: none -> 40.6 us  [per_device(): lax.all_gather(jnp.sum(mixed_sum * mixed_sum, axis=1), ('kv', 'tp'))]
    psum x1 -> x0, blocking collectives: 39.3 us -> none  [per_device(): squares = lax.psum(jnp.sum(mixed_sum * mixed_sum, axis=1), ('kv', 'tp'))]
  transfers between devices with their start and end apart: 3 -> 3, of which waited for: 2 -> 2; matrix products, arithmetic and copies ran while one was open for 7% -> 6% of each run, Pallas kernels for 0% -> 0%
where the time goes in v1:
time: 296 us; the launch traced here: 295 us
  blocking collectives  131 us (44%)
  waiting for transfers between devices  87 us (29%)
  local copies, waits for them, and re-layouts  25.7 us (9%)
  other arithmetic  19.8 us (7%)
  matrix products  16.7 us (6%)
  between operations  14.2 us (5%)
    all_gather x3, blocking collectives, merged(): gathered = jax.tree.map(lambda a: lax.all_gather(a, axis), part)  90.6 us
    psum x1, waiting for transfers between devices, per_device(): lax.psum(key_part.astype(jnp.bfloat16), 'kv').astype(jnp.float32)  75.1 us
    all_gather x1, blocking collectives, per_device(): lax.all_gather(jnp.sum(mixed_sum * mixed_sum, axis=1), ('kv', 'tp'))  40.6 us
    unnamed x4, waiting for transfers between devices  11.8 us
    unnamed x42, local copies, waits for them, and re-layouts  8.8 us
    dynamic_slice x11, local copies, waits for them, and re-layouts, take(): lax.dynamic_index_in_dim(a, source, 0, False)  8.64 us
    add x7, other arithmetic, combine_parts(): first[2] * first_scale[..., None] + second[2] * second_scale[..., None]  6.66 us
  transfers between devices with their start and end apart: 3, of which 2 were waited for; matrix products, arithmetic and copies ran while one was open for 6% of the time, Pallas kernels for 0%

profile of v1, /device:TPU:0, one launch (start us, length us, event | category | flops | bytes accessed | tf_op | source)
XLA Modules:
  0.0 295.0 jit_solution(3005657629722579693)
XLA Ops:
  7.2 2.1 fusion.4
  9.4 2.2 fusion.6
  12.8 1.3 convolution_convert_fusion.1
  14.2 1.4 convolution_convert_fusion.3
  18.0 1.5 fusion.71
  20.6 75.1 %all-reduce.3.cloned.1.call-done = (bf16[16,16,4,128]{3,1,2,0:T(8,128)(2,1)}, bf16[16,16,4,128]{3,1,2,0:T(8,128)(2,1)}, bf16[16,16,4,128]{3,1,2,0:T(8,128)(2,1)}) async-done(((bf16[16,16,4,128]{3,1,2,0:T(8,128)(2,1)}, bf16[16,16,4,128]{3,1,2,0:T(8,128)(2,1)}, bf16[16,16,4,128]{3,1,2,0:T(8,128)(2,1)}), (bf16[16,16,4,128]{3,1,2,0:T(8,128)(2,1)}, bf16[16,16,4,128]{3,1,2,0:T(8,128)(2,1)}, ...) | async-done | bytes 786448 | tf_op jit(solution)/shard_map/psum | solution.py:97
  95.7 3.0 %select_reduce_fusion.1 = (f32[16,16,4]{1,2,0:T(4,128)S(1)}, f32[16,16,4,128]{3,1,2,0:T(8,128)S(1)}) fusion(pred[16,128]{1,0:T(8,128)(4,1)S(1)} %get-tuple-element.314, f32[16,4,128]{2,1,0:T(4,128)S(1)} %bitcast.133, f32[16,16,4]{1,2,0:T(4,128)S(1)} %fusion.63, bf16[16,16,4,128]{3,1,2,0:T(8,128)(2,1)} %get-tuple-element.302, ...), kind=kOutput, calls=%fused_computation.51 | convolution fusion | flops 34208768 | bytes 2926592 | tf_op jit(solution)/shard_map/bihd,bkhd->bihk/dot_general | solution.py:117
  99.5 1.5 fusion.11
  101.4 26.7 %all-gather.5 = f32[8,16,4]{1,2,0:T(4,128)S(1)} all-gather(f32[1,16,4]{1,2,0:T(4,128)S(1)} %bitcast.135), channel_id=5, replica_groups=mesh['kv'=8,'tp'=4] {'kv'}, dimensions={0}, use_global_device_ids=true | all-gather | bytes 2304 | tf_op jit(solution)/shard_map/all_gather | solution.py:11
  128.8 1.4 select_reduce_fusion
  131.9 32.2 %all-gather = f32[128,16,4]{1,2,0:T(4,128)S(1)} all-gather(f32[16,16,4]{1,2,0:T(4,128)S(1)} %get-tuple-element.320), channel_id=2, replica_groups=mesh['kv'=8,'tp'=4] {'kv'}, dimensions={0}, use_global_device_ids=true | all-gather | bytes 36864 | tf_op jit(solution)/shard_map/all_gather | solution.py:11
  164.1 1.5 fusion.33
  165.6 31.7 %all-gather.1 = f32[128,16,4]{1,2,0:T(4,128)S(1)} all-gather(f32[16,16,4]{1,2,0:T(4,128)S(1)} %fusion.33), channel_id=3, replica_groups=mesh['kv'=8,'tp'=4] {'kv'}, dimensions={0}, use_global_device_ids=true | all-gather | bytes 36864 | tf_op jit(solution)/shard_map/all_gather | solution.py:11
  198.3 3.1 %copy.110 = bf16[16,128,4,128]{3,2,1,0:T(4,128)(2,1)} copy(bf16[16,128,4,128]{3,1,2,0:T(8,128)(2,1)S(1)} %convert_select_fusion) | data formatting | bytes 4194304
  202.6 22.1 %while.21 = (s32[]{:T(128)}, f32[16,16,4]{1,2,0:T(4,128)S(1)}, f32[16,16,4]{1,2,0:T(4,128)S(1)}, f32[16,16,4,128]{3,2,1,0:T(4,128)S(1)}, f32[16,4]{0,1:T(4,128)S...) while((s32[]{:T(128)}, f32[16,16,4]{1,2,0:T(4,128)S(1)}, ...), condition=%wide.region_6.7_spmd, body=%wide.region_5.6_spmd.sunk | while | flops 399429 | bytes 2679715 | solution.py:16
  203.8 1.1 constant_dynamic-slice_fusion.2
  206.9 1.1 constant_dynamic-slice_fusion.2
  210.1 1.1 constant_dynamic-slice_fusion.2
  213.2 1.1 constant_dynamic-slice_fusion.2
  216.4 1.1 constant_dynamic-slice_fusion.2
  227.8 2.4 convert_select_fusion.1
  230.2 3.1 %copy.109 = bf16[16,128,4,128]{3,2,1,0:T(4,128)(2,1)} copy(bf16[16,128,4,128]{3,1,2,0:T(8,128)(2,1)S(1)} %convert_select_fusion.1) | data formatting | bytes 4194304
  234.2 11.8 %reduce-scatter.4.cloned.1.call-done = bf16[128,256]{1,0:T(8,128)(2,1)} async-done(((bf16[512,256]{1,0:T(8,128)(2,1)}), bf16[128,256]{1,0:T(8,128)(2,1)}) %reduce-scatter.4.cloned.1.call-update) | async-done | bytes 65552
  247.1 40.6 %all-gather.6 = f32[32,1,256]{2,1,0:T(1,128)S(1)} all-gather(f32[1,1,256]{2,1,0:T(1,128)S(1)} %bitcast.136), channel_id=6, replica_groups=mesh['kv'=8,'tp'=4] {'kv','tp'}, dimensions={0}, use_global_device_ids=true | all-gather | bytes 33792 | tf_op jit(solution)/shard_map/all_gather | solution.py:169
  (139 shorter events, 32.6 us)
Async XLA Ops:
  7.2 4.5 %copy-start = (bf16[512,512]{1,0:T(8,128)(2,1)S(1)}, bf16[512,512]{1,0:T(8,128)(2,1)}, u32[]{:S(2)}) copy-start(bf16[512,512]{1,0:T(8,128)(2,1)} %param.20) | copy-start | bytes 1572868
  7.2 2.2 copy-start.10
  7.2 88.5 %all-reduce.3.cloned.1.call-start = ((), (), s32[]{:S(2)}) async-start(), calls=%async_computation.3 | async-start | bytes 1572864 | tf_op jit(solution)/shard_map/psum | solution.py:97
  14.1 3.2 %copy-start.17 = (s32[16,16]{1,0:T(8,128)S(1)}, s32[16,16]{1,0:T(8,128)}, u32[]{:S(2)}) copy-start(s32[16,16]{1,0:T(8,128)} %param.31) | copy-start | bytes 3076
  14.1 3.8 %copy-start.18 = (f32[16]{0:T(128)S(1)}, f32[16]{0:T(128)}, u32[]{:S(2)}) copy-start(f32[16]{0:T(128)} %param.23) | copy-start | bytes 196
  14.1 3.9 %copy-start.13 = (s32[16]{0:T(128)S(1)}, s32[16]{0:T(128)}, u32[]{:S(2)}) copy-start(s32[16]{0:T(128)} %param.29) | copy-start | bytes 196
  14.1 3.9 %copy-start.14 = (s32[16]{0:T(128)S(1)}, s32[16]{0:T(128)}, u32[]{:S(2)}) copy-start(s32[16]{0:T(128)} %param.30) | copy-start | bytes 196
  17.2 78.5 %copy-start.6 = (f32[16,128,4]{1,2,0:T(4,128)S(1)}, f32[16,128,4]{1,2,0:T(4,128)}, u32[]{:S(2)}) copy-start(f32[16,128,4]{1,2,0:T(4,128)} %param.28) | copy-start | bytes 98308
  17.2 184.2 %all-gather.9.cloned.1.call-start = ((), (), s32[]{:S(2)}) async-start(), calls=%async_computation.1 | async-start | bytes 4718592 | tf_op jit(solution)/shard_map/all_gather | solution.py:11
  19.7 79.8 %copy-start.1 = (bf16[16,128,4,128]{3,2,1,0:T(4,128)(2,1)S(1)}, bf16[16,128,4,128]{3,2,1,0:T(4,128)(2,1)}, u32[]{:S(2)}) copy-start(bf16[16,128,4,128]{3,2,1,0:T(4,128)(2,1)} %param.27) | copy-start | bytes 6291460
  20.5 108.2 %copy-start.8 = (f32[16,16,4]{1,2,0:T(4,128)}, f32[16,16,4]{1,2,0:T(4,128)S(1)}, u32[]{:S(2)}) copy-start(f32[16,16,4]{1,2,0:T(4,128)S(1)} %fusion.63) | copy-start | bytes 12292
  98.7 0.8 copy-start.2
  99.5 30.7 %copy-start.4 = (bf16[16,16,4,128]{3,1,2,0:T(8,128)(2,1)S(1)}, bf16[16,16,4,128]{3,1,2,0:T(8,128)(2,1)}, u32[]{:S(2)}) copy-start(bf16[16,16,4,128]{3,1,2,0:T(8,128)(2,1)} %get-tuple-element.303) | copy-start | bytes 786436
  101.0 144.9 %reduce-scatter.4.cloned.1.call-start = ((), (), s32[]{:S(2)}) async-start(), calls=%async_computation.2 | async-start | bytes 327680
  128.1 0.7 copy-start.5
  130.2 67.0 %copy-start.11 = (s32[16,128]{1,0:T(8,128)S(1)}, s32[16,128]{1,0:T(8,128)}, u32[]{:S(2)}) copy-start(s32[16,128]{1,0:T(8,128)} %broadcast_subtract_fusion) | copy-start | bytes 24580
  224.7 1.9 copy-start.3
  224.8 1.8 copy-start.15
  226.6 1.2 copy-start.16
  230.2 3.1 %copy-start.7 = (f32[16,128,4]{1,2,0:T(4,128)S(1)}, f32[16,128,4]{1,2,0:T(4,128)}, u32[]{:S(2)}) copy-start(f32[16,128,4]{1,2,0:T(4,128)} %param.28) | copy-start | bytes 98308
  230.2 3.1 %copy-start.9 = (f32[16,16,4]{1,2,0:T(4,128)S(1)}, f32[16,16,4]{1,2,0:T(4,128)}, u32[]{:S(2)}) copy-start(f32[16,16,4]{1,2,0:T(4,128)} %copy-done.8) | copy-start | bytes 12292
  230.2 57.5 %copy-start.12 = (f32[128]{0:T(128)S(1)}, f32[128]{0:T(128)}, u32[]{:S(2)}) copy-start(f32[128]{0:T(128)} %param.25) | copy-start | bytes 1540
Sparse Core Ops, SparseCore 0:
  17.3 78.3 all-reduce.2
  101.2 77.8 all-gather.8
  228.0 17.9 reduce-scatter.3
